TPU v7x, 32 devices: a whole 2x2x4 slice. The times are simulated.
32 devices in a mesh: grp: 2 (over y), ra: 4 (over z), cb: 2 (over x), dp: 2 (over core).
Axes of the slice: x: 2, y: 2, z: 4, core: 2. Of those that a mesh axis runs over, the one named last changes fastest.
Arguments:
- tokens: bfloat16 [256, 2048], P(('grp', 'dp'), 'ra'), parts along dimension 0, may hold values from -62 to 62
- gain_first: float32 [2048], P('ra'), may hold values from 0.1 to 1.9
- up_first: bfloat16 [2048, 8192], P('ra', 'cb'), may hold values from -0.125 to 0.125
- down_first: bfloat16 [8192, 2048], P('cb', 'ra'), may hold values from -0.0625 to 0.0625
- gain_second: float32 [2048], P('ra'), may hold values from 0.1 to 1.9
- up_second: bfloat16 [2048, 8192], P('ra', 'cb'), may hold values from -0.125 to 0.125
- down_second: bfloat16 [8192, 2048], P('cb', 'ra'), may hold values from -0.0625 to 0.0625
- gain_last: float32 [2048], P('ra'), may hold values from 0.1 to 1.9
Outputs:
- normed: bfloat16 [256, 2048], P(('grp', 'dp'), 'ra'), parts along dimension 0
There are 2 independent parts, one for each index of `grp`. A program takes and returns all parts, laid end to end along the dimension named above; an argument that names none is the same for every part. Nothing has to cross between parts.
All inputs are finite; a program needn't handle non-finite values.
Results may differ from a plain program's by a relative error of at most 0.0095.
Values may be sent and summed in bfloat16 or wider, within the bound.
A program may use at most 64 MiB of HBM per device.

v0:
```python
import jax
import jax.numpy as jnp
from jax import lax
from jax.sharding import PartitionSpec as P

D = 2048
EPS = 1e-06


def squares_inverse(h32):
    local_sq = jnp.sum(h32 * h32, axis=1)
    summed_sq = lax.psum(local_sq, "ra")
    return lax.rsqrt(summed_sq / D + EPS)


def activate(summed, inverse):
    return jnp.square(jax.nn.relu(summed * inverse[:, None])).astype(jnp.bfloat16)


def mlp_branch(h32, gain, w_up, w_down):
    scaled = (h32 * gain).astype(jnp.bfloat16)
    partial_value = jnp.dot(scaled, w_up, preferred_element_type=jnp.float32)
    inverse = squares_inverse(h32)
    shared = lax.psum_scatter(partial_value, "ra", scatter_dimension=1, tiled=True)
    hidden_share = activate(shared, inverse)
    down = jnp.dot(
        lax.all_gather(hidden_share, "ra", axis=1, tiled=True),
        w_down,
        preferred_element_type=jnp.float32,
    )
    return lax.psum(down, "cb")


def local(tokens, gain_first, up_first, down_first, gain_second, up_second, down_second, gain_last):
    start32 = tokens.astype(jnp.float32)
    first = (0.5 * start32 + mlp_branch(start32, gain_first, up_first, down_first)).astype(
        jnp.bfloat16
    )
    first32 = first.astype(jnp.float32)
    second = (0.5 * first32 + mlp_branch(first32, gain_second, up_second, down_second)).astype(
        jnp.bfloat16
    )
    second32 = second.astype(jnp.float32)
    inverse = squares_inverse(second32)
    return (second32 * inverse[:, None] * gain_last).astype(jnp.bfloat16)


def solution(mesh):
    return jax.shard_map(
        local,
        mesh=mesh,
        in_specs=(
            P(("grp", "dp"), "ra"),
            P("ra"),
            P("ra", "cb"),
            P("cb", "ra"),
            P("ra"),
            P("ra", "cb"),
            P("cb", "ra"),
            P("ra"),
        ),
        out_specs=P(("grp", "dp"), "ra"),
        check_vma=False,
    )
```

profile of v0, /device:TPU:0, one launch (start us, length us, event | category | flops | bytes accessed | tf_op | source)
XLA Modules:
  0.0 175.9 jit_solution(10254012345547402609)
XLA Ops:
  6.5 0.0 copy-start
  6.5 0.0 reduce-scatter.3.cloned.1.call-start
  6.5 4.1 %fusion.13 = f32[64,4096]{1,0:T(8,128)} fusion(bf16[512,4096]{1,0:T(8,128)(2,1)} %param.10, bf16[64,512]{1,0:T(8,128)(2,1)} %param.8, f32[512]{0:T(512)} %param.9), kind=kOutput, calls=%fused_computation.22 | convolution fusion | flops 268533760 | bytes 5310464 | tf_op jit(solution)/shard_map/dot_general | solution.py:22
  10.6 0.0 copy-start.1
  10.7 0.0 reduce-scatter.3.cloned.1.call-update
  10.7 0.0 all-reduce.3.cloned.1.call-start
  10.7 0.0 copy-done
  10.7 0.1 fusion.6
  10.8 13.5 %psum.35 = f32[64]{0:T(128)S(1)} all-reduce(f32[64]{0:T(128)S(1)} %fusion.6), channel_id=1, replica_groups=mesh['grp'=2,'ra'=4,'cb'=2,'dp'=2] {'ra'}, use_global_device_ids=true, to_apply=%region_2.0 | all-reduce | flops 64 | bytes 512 | tf_op jit(solution)/shard_map/psum | solution.py:12
  24.4 16.5 %reduce-scatter.3.cloned.1.call-done = f32[64,1024]{1,0:T(8,128)} async-done(((f32[64,4096]{1,0:T(8,128)}), f32[64,1024]{1,0:T(8,128)}) %reduce-scatter.3.cloned.1.call-update) | async-done | bytes 262160 | tf_op jit(solution)/shard_map/reduce_scatter | solution.py:24
  40.9 1.0 multiply_convert_fusion.1
  41.9 15.9 %all_gather.6 = bf16[64,4096]{1,0:T(8,128)(2,1)S(1)} all-gather(bf16[64,1024]{1,0:T(8,128)(2,1)S(1)} %multiply_convert_fusion.1), channel_id=1, replica_groups=mesh['grp'=2,'ra'=4,'cb'=2,'dp'=2] {'ra'}, dimensions={1}, use_global_device_ids=true | all-gather | bytes 655360 | tf_op jit(solution)/shard_map/all_gather | solution.py:27
  57.8 3.7 %fusion.18 = f32[64,512]{1,0:T(8,128)} fusion(bf16[64,4096]{1,0:T(8,128)(2,1)S(1)} %all_gather.6, bf16[4096,512]{1,0:T(8,128)(2,1)} %param.11), kind=kOutput, calls=%fused_computation.28 | convolution fusion | flops 268435456 | bytes 4849664 | tf_op jit(solution)/shard_map/dot_general | solution.py:26
  61.5 0.0 all-reduce.3.cloned.1.call-update
  61.5 0.0 reduce-scatter.5.cloned.1.call-start
  61.6 20.1 %all-reduce.3.cloned.1.call-done = f32[64,512]{1,0:T(8,128)} async-done(((f32[64,512]{1,0:T(8,128)}), f32[64,512]{1,0:T(8,128)}) %all-reduce.3.cloned.1.call-update) | async-done | bytes 131088 | tf_op jit(solution)/shard_map/psum | solution.py:31
  81.7 1.0 fusion.10
  82.7 0.0 copy-done.1
  82.7 4.0 %fusion.11 = f32[64,4096]{1,0:T(8,128)} fusion(bf16[512,4096]{1,0:T(8,128)(2,1)} %param.13, bf16[64,512]{1,0:T(8,128)(2,1)S(1)} %get-tuple-element.6, f32[512]{0:T(512)S(1)} %copy-done.1), kind=kOutput, calls=%fused_computation.21 | convolution fusion | flops 268533760 | bytes 5310464 | tf_op jit(solution)/shard_map/dot_general | solution.py:22
  86.7 0.0 reduce-scatter.5.cloned.1.call-update
  86.8 0.0 all-reduce.5.cloned.1.call-start
  86.8 11.9 %psum.37 = f32[64]{0:T(128)S(1)} all-reduce(f32[64]{0:T(128)S(1)} %get-tuple-element.5), channel_id=1, replica_groups=mesh['grp'=2,'ra'=4,'cb'=2,'dp'=2] {'ra'}, use_global_device_ids=true, to_apply=%region_6.7 | all-reduce | flops 64 | bytes 512 | tf_op jit(solution)/shard_map/psum | solution.py:12
  98.7 15.6 %reduce-scatter.5.cloned.1.call-done = f32[64,1024]{1,0:T(8,128)} async-done(((f32[64,4096]{1,0:T(8,128)}), f32[64,1024]{1,0:T(8,128)}) %reduce-scatter.5.cloned.1.call-update) | async-done | bytes 262160 | tf_op jit(solution)/shard_map/reduce_scatter | solution.py:24
  114.3 1.0 multiply_convert_fusion
  115.3 15.9 %all_gather.7 = bf16[64,4096]{1,0:T(8,128)(2,1)S(1)} all-gather(bf16[64,1024]{1,0:T(8,128)(2,1)S(1)} %multiply_convert_fusion), channel_id=1, replica_groups=mesh['grp'=2,'ra'=4,'cb'=2,'dp'=2] {'ra'}, dimensions={1}, use_global_device_ids=true | all-gather | bytes 655360 | tf_op jit(solution)/shard_map/all_gather | solution.py:27
  131.2 3.7 %fusion.19 = f32[64,512]{1,0:T(8,128)} fusion(bf16[64,4096]{1,0:T(8,128)(2,1)S(1)} %all_gather.7, bf16[4096,512]{1,0:T(8,128)(2,1)} %param.14), kind=kOutput, calls=%fused_computation.29 | convolution fusion | flops 268435456 | bytes 4849664 | tf_op jit(solution)/shard_map/dot_general | solution.py:26
  134.9 0.0 all-reduce.5.cloned.1.call-update
  134.9 20.1 %all-reduce.5.cloned.1.call-done = f32[64,512]{1,0:T(8,128)} async-done(((f32[64,512]{1,0:T(8,128)}), f32[64,512]{1,0:T(8,128)}) %all-reduce.5.cloned.1.call-update) | async-done | bytes 131088 | tf_op jit(solution)/shard_map/psum | solution.py:31
  155.0 1.0 fusion
  156.0 11.7 %psum.39 = f32[64]{0:T(128)S(1)} all-reduce(f32[64]{0:T(128)S(1)} %fusion), channel_id=1, replica_groups=mesh['grp'=2,'ra'=4,'cb'=2,'dp'=2] {'ra'}, use_global_device_ids=true, to_apply=%region_9.10 | all-reduce | flops 64 | bytes 512 | tf_op jit(solution)/shard_map/psum | solution.py:12
  167.7 0.0 copy-done.2
  167.7 1.6 fusion.2
  (4 shorter events, 0.0 us)
Async XLA Ops:
  6.5 4.2 %copy-start = (bf16[64,512]{1,0:T(8,128)(2,1)S(1)}, bf16[64,512]{1,0:T(8,128)(2,1)}, u32[]{:S(2)}) copy-start(bf16[64,512]{1,0:T(8,128)(2,1)} %param.8) | copy-start | bytes 196612
  6.5 34.4 %reduce-scatter.3.cloned.1.call-start = ((), (), s32[]{:S(2)}) async-start(), calls=%async_computation.2 | async-start | bytes 1310720 | tf_op jit(solution)/shard_map/reduce_scatter | solution.py:24
  10.6 72.1 %copy-start.1 = (f32[512]{0:T(512)S(1)}, f32[512]{0:T(512)}, u32[]{:S(2)}) copy-start(f32[512]{0:T(512)} %param.12) | copy-start | bytes 6148
  10.7 71.0 %all-reduce.3.cloned.1.call-start = ((), (), s32[]{:S(2)}) async-start(), calls=%async_computation.3 | async-start | bytes 262144 | tf_op jit(solution)/shard_map/psum | solution.py:31
  61.5 52.7 %reduce-scatter.5.cloned.1.call-start = ((), (), s32[]{:S(2)}) async-start(), calls=%async_computation.4 | async-start | bytes 1310720 | tf_op jit(solution)/shard_map/reduce_scatter | solution.py:24
  86.7 81.0 %copy-start.2 = (f32[512]{0:T(512)S(1)}, f32[512]{0:T(512)}, u32[]{:S(2)}) copy-start(f32[512]{0:T(512)} %param.15) | copy-start | bytes 6148
  86.8 68.2 %all-reduce.5.cloned.1.call-start = ((), (), s32[]{:S(2)}) async-start(), calls=%async_computation.5 | async-start | bytes 262144 | tf_op jit(solution)/shard_map/psum | solution.py:31
Sparse Core Ops, SparseCore 0:
  10.8 30.0 reduce-scatter.2
  61.7 19.9 all-reduce.2
  86.9 27.3 reduce-scatter.4
  135.0 19.9 all-reduce.4
where the time goes:
time: 176 us
  waiting for transfers between devices  72.4 us (41%)
  blocking collectives  68.8 us (39%)
  matrix products  15.5 us (9%)
  between operations  13.2 us (8%)
  other arithmetic  5.91 us (3%)
    psum x2, waiting for transfers between devices, mlp_branch(): return lax.psum(down, 'cb')  40.2 us
    psum x3, blocking collectives, squares_inverse(): summed_sq = lax.psum(local_sq, 'ra')  37 us
    reduce_scatter x2, waiting for transfers between devices, mlp_branch(): lax.psum_scatter(partial_value, 'ra', scatter_dimension=1, tiled=True)  32.1 us
    all_gather x2, blocking collectives, mlp_branch(): lax.all_gather(hidden_share, 'ra', axis=1, tiled=True)  31.8 us
    dot_general x2, matrix products, mlp_branch(): partial_value = jnp.dot(scaled, w_up, preferred_element_type=jnp.float32)  8.13 us
    dot_general x2, matrix products, mlp_branch(): jnp.dot(lax.all_gather(hidden_share, 'ra', axis=1, tiled=True), w_down, p...  7.35 us
  transfers between devices with their start and end apart: 4, of which 4 were waited for; matrix products, arithmetic and copies ran while one was open for 0% of the time, Pallas kernels for 0%

commit v1 on v0

--- a/solution.py
+++ b/solution.py
@@ -28,7 +28,7 @@
         w_down,
         preferred_element_type=jnp.float32,
     )
-    return lax.psum(down, "cb")
+    return jnp.sum(lax.all_gather(down, "cb"), axis=0)
 
 
 def local(tokens, gain_first, up_first, down_first, gain_second, up_second, down_second, gain_last):

time: 176 us -> 139 us (0.79)
  waiting for transfers between devices: 72.4 us -> 34 us
  blocking collectives: 68.8 us -> 73.5 us
  other arithmetic: 5.91 us -> 3.23 us
    psum x2 -> x0, waiting for transfers between devices: 40.2 us -> none  [mlp_branch(): return lax.psum(down, 'cb')]
    all_gather x0 -> x2, blocking collectives: none -> 11.3 us  [mlp_branch(): return jnp.sum(lax.all_gather(down, 'cb'), axis=0)]
    psum x3, blocking collectives: 37 us -> 30.3 us  [squares_inverse(): summed_sq = lax.psum(local_sq, 'ra')]
    reduce_scatter x2, waiting for transfers between devices: 32.1 us -> 34 us  [mlp_branch(): lax.psum_scatter(partial_value, 'ra', scatter_dimension=1, tiled=True)]
    reduce_sum x3, other arithmetic: 2.17 us -> 0.36 us  [squares_inverse(): local_sq = jnp.sum(h32 * h32, axis=1)]
  transfers between devices with their start and end apart: 4 -> 2, of which waited for: 4 -> 2; matrix products, arithmetic and copies ran while one was open for 0% -> 0% of each run, Pallas kernels for 0% -> 0%
where the time goes in v1:
time: 139 us; the launch traced here: 138 us
  blocking collectives  73.5 us (53%)
  waiting for transfers between devices  34 us (24%)
  matrix products  14.2 us (10%)
  between operations  13.4 us (10%)
  other arithmetic  3.23 us (2%)
    reduce_scatter x2, waiting for transfers between devices, mlp_branch(): lax.psum_scatter(partial_value, 'ra', scatter_dimension=1, tiled=True)  34 us
    all_gather x2, blocking collectives, mlp_branch(): lax.all_gather(hidden_share, 'ra', axis=1, tiled=True)  31.9 us
    psum x3, blocking collectives, squares_inverse(): summed_sq = lax.psum(local_sq, 'ra')  30.3 us
    all_gather x2, blocking collectives, mlp_branch(): return jnp.sum(lax.all_gather(down, 'cb'), axis=0)  11.3 us
    dot_general x2, matrix products, mlp_branch(): partial_value = jnp.dot(scaled, w_up, preferred_element_type=jnp.float32)  8.13 us
    dot_general x2, matrix products, mlp_branch(): jnp.dot(lax.all_gather(hidden_share, 'ra', axis=1, tiled=True), w_down, p...  6.03 us
  transfers between devices with their start and end apart: 2, of which 2 were waited for; matrix products, arithmetic and copies ran while one was open for 0% of the time, Pallas kernels for 0%

profile of v1, /device:TPU:0, one launch (start us, length us, event | category | flops | bytes accessed | tf_op | source)
XLA Modules:
  0.0 138.4 jit_solution(15788777601323606918)
XLA Ops:
  6.5 0.0 copy-start
  6.5 0.0 reduce-scatter.3.cloned.1.call-start
  6.5 4.1 %fusion.13 = f32[64,4096]{1,0:T(8,128)} fusion(bf16[512,4096]{1,0:T(8,128)(2,1)} %param.10, bf16[64,512]{1,0:T(8,128)(2,1)} %param.8, f32[512]{0:T(512)} %param.9), kind=kOutput, calls=%fused_computation.22 | convolution fusion | flops 268533760 | bytes 5310464 | tf_op jit(solution)/shard_map/dot_general | solution.py:22
  10.6 0.0 copy-start.1
  10.7 0.0 reduce-scatter.3.cloned.1.call-update
  10.7 0.0 reduce-scatter.5.cloned.1.call-start
  10.7 0.0 copy-done
  10.7 0.1 fusion.6
  10.8 13.5 %psum.21 = f32[64]{0:T(128)S(1)} all-reduce(f32[64]{0:T(128)S(1)} %fusion.6), channel_id=1, replica_groups=mesh['grp'=2,'ra'=4,'cb'=2,'dp'=2] {'ra'}, use_global_device_ids=true, to_apply=%region_2.0 | all-reduce | flops 64 | bytes 512 | tf_op jit(solution)/shard_map/psum | solution.py:12
  24.4 16.5 %reduce-scatter.3.cloned.1.call-done = f32[64,1024]{1,0:T(8,128)} async-done(((f32[64,4096]{1,0:T(8,128)}), f32[64,1024]{1,0:T(8,128)}) %reduce-scatter.3.cloned.1.call-update) | async-done | bytes 262160 | tf_op jit(solution)/shard_map/reduce_scatter | solution.py:24
  40.9 1.0 multiply_convert_fusion.1
  41.9 15.9 %all_gather.18 = bf16[64,4096]{1,0:T(8,128)(2,1)S(1)} all-gather(bf16[64,1024]{1,0:T(8,128)(2,1)S(1)} %multiply_convert_fusion.1), channel_id=1, replica_groups=mesh['grp'=2,'ra'=4,'cb'=2,'dp'=2] {'ra'}, dimensions={1}, use_global_device_ids=true | all-gather | bytes 655360 | tf_op jit(solution)/shard_map/all_gather | solution.py:27
  57.8 3.0 %fusion.18 = f32[64,512]{1,0:T(8,128)S(1)} fusion(bf16[64,4096]{1,0:T(8,128)(2,1)S(1)} %all_gather.18, bf16[4096,512]{1,0:T(8,128)(2,1)} %param.11), kind=kOutput, calls=%fused_computation.28 | convolution fusion | flops 268435456 | bytes 4849664 | tf_op jit(solution)/shard_map/dot_general | solution.py:26
  60.9 5.6 %all-gather = f32[128,512]{1,0:T(8,128)S(1)} all-gather(f32[64,512]{1,0:T(8,128)S(1)} %fusion.18), channel_id=2, replica_groups=mesh['grp'=2,'ra'=4,'cb'=2,'dp'=2] {'cb'}, dimensions={0}, use_global_device_ids=true | all-gather | bytes 393216 | tf_op jit(solution)/shard_map/all_gather | solution.py:31
  66.5 0.1 fusion.10
  66.6 0.0 copy-done.1
  66.6 4.0 %fusion.11 = f32[64,4096]{1,0:T(8,128)} fusion(bf16[512,4096]{1,0:T(8,128)(2,1)} %param.13, bf16[64,512]{1,0:T(8,128)(2,1)S(1)} %get-tuple-element.6, f32[512]{0:T(512)S(1)} %copy-done.1), kind=kOutput, calls=%fused_computation.21 | convolution fusion | flops 268533760 | bytes 5310464 | tf_op jit(solution)/shard_map/dot_general | solution.py:22
  70.7 0.0 copy-start.2
  70.7 0.0 reduce-scatter.5.cloned.1.call-update
  70.7 8.5 %psum.22 = f32[64]{0:T(128)S(1)} all-reduce(f32[64]{0:T(128)S(1)} %get-tuple-element.5), channel_id=1, replica_groups=mesh['grp'=2,'ra'=4,'cb'=2,'dp'=2] {'ra'}, use_global_device_ids=true, to_apply=%region_6.7 | all-reduce | flops 64 | bytes 512 | tf_op jit(solution)/shard_map/psum | solution.py:12
  79.2 17.4 %reduce-scatter.5.cloned.1.call-done = f32[64,1024]{1,0:T(8,128)} async-done(((f32[64,4096]{1,0:T(8,128)}), f32[64,1024]{1,0:T(8,128)}) %reduce-scatter.5.cloned.1.call-update) | async-done | bytes 262160 | tf_op jit(solution)/shard_map/reduce_scatter | solution.py:24
  96.6 1.0 multiply_convert_fusion
  97.7 16.0 %all_gather.21 = bf16[64,4096]{1,0:T(8,128)(2,1)S(1)} all-gather(bf16[64,1024]{1,0:T(8,128)(2,1)S(1)} %multiply_convert_fusion), channel_id=1, replica_groups=mesh['grp'=2,'ra'=4,'cb'=2,'dp'=2] {'ra'}, dimensions={1}, use_global_device_ids=true | all-gather | bytes 655360 | tf_op jit(solution)/shard_map/all_gather | solution.py:27
  113.6 3.0 %fusion.19 = f32[64,512]{1,0:T(8,128)S(1)} fusion(bf16[64,4096]{1,0:T(8,128)(2,1)S(1)} %all_gather.21, bf16[4096,512]{1,0:T(8,128)(2,1)} %param.14), kind=kOutput, calls=%fused_computation.29 | convolution fusion | flops 268435456 | bytes 4849664 | tf_op jit(solution)/shard_map/dot_general | solution.py:26
  116.6 5.6 %all-gather.1 = f32[128,512]{1,0:T(8,128)S(1)} all-gather(f32[64,512]{1,0:T(8,128)S(1)} %fusion.19), channel_id=3, replica_groups=mesh['grp'=2,'ra'=4,'cb'=2,'dp'=2] {'cb'}, dimensions={0}, use_global_device_ids=true | all-gather | bytes 393216 | tf_op jit(solution)/shard_map/all_gather | solution.py:31
  122.3 0.1 fusion
  122.4 8.4 %psum.23 = f32[64]{0:T(128)S(1)} all-reduce(f32[64]{0:T(128)S(1)} %fusion), channel_id=1, replica_groups=mesh['grp'=2,'ra'=4,'cb'=2,'dp'=2] {'ra'}, use_global_device_ids=true, to_apply=%region_9.10 | all-reduce | flops 64 | bytes 512 | tf_op jit(solution)/shard_map/psum | solution.py:12
  130.8 0.0 copy-done.2
  130.8 0.7 fusion.2
  (5 shorter events, 0.1 us)
Async XLA Ops:
  6.5 4.2 %copy-start = (bf16[64,512]{1,0:T(8,128)(2,1)S(1)}, bf16[64,512]{1,0:T(8,128)(2,1)}, u32[]{:S(2)}) copy-start(bf16[64,512]{1,0:T(8,128)(2,1)} %param.8) | copy-start | bytes 196612
  6.5 34.4 %reduce-scatter.3.cloned.1.call-start = ((), (), s32[]{:S(2)}) async-start(), calls=%async_computation.2 | async-start | bytes 1310720 | tf_op jit(solution)/shard_map/reduce_scatter | solution.py:24
  10.6 56.0 %copy-start.1 = (f32[512]{0:T(512)S(1)}, f32[512]{0:T(512)}, u32[]{:S(2)}) copy-start(f32[512]{0:T(512)} %param.12) | copy-start | bytes 6148
  10.7 85.9 %reduce-scatter.5.cloned.1.call-start = ((), (), s32[]{:S(2)}) async-start(), calls=%async_computation.3 | async-start | bytes 1310720 | tf_op jit(solution)/shard_map/reduce_scatter | solution.py:24
  70.7 60.1 %copy-start.2 = (f32[512]{0:T(512)S(1)}, f32[512]{0:T(512)}, u32[]{:S(2)}) copy-start(f32[512]{0:T(512)} %param.15) | copy-start | bytes 6148
Sparse Core Ops, SparseCore 0:
  10.8 30.0 reduce-scatter.2
  70.8 25.7 reduce-scatter.4
